TPU v7x, 32 devices: a whole 2x2x4 slice. The times are simulated.
32 devices in a mesh: fs: 16 (over z, y, x), tp: 2 (over core).
Axes of the slice: x: 2, y: 2, z: 4, core: 2. Of those that a mesh axis runs over, the one named last changes fastest.
Arguments:
- tokens: bfloat16 [6144, 2048], P('fs'), may hold values from -6 to 6
- merged: bfloat16 [6144, 2048], P('fs'), may hold values from -6 to 6
- gain_first: float32 [2048], replicated, may hold values from 0.1 to 1.9
- gate_first: bfloat16 [2048, 2816], P('fs', 'tp'), may hold values from -0.125 to 0.125
- up_first: bfloat16 [2048, 2816], P('fs', 'tp'), may hold values from -0.125 to 0.125
- down_first: bfloat16 [2816, 2048], P('tp', 'fs'), may hold values from -0.21875 to 0.21875
- gain_second: float32 [2048], replicated, may hold values from 0.1 to 1.9
- gate_second: bfloat16 [2048, 2816], P('fs', 'tp'), may hold values from -0.125 to 0.125
- up_second: bfloat16 [2048, 2816], P('fs', 'tp'), may hold values from -0.125 to 0.125
- down_second: bfloat16 [2816, 2048], P('tp', 'fs'), may hold values from -0.21875 to 0.21875
Outputs:
- result: bfloat16 [6144, 2048], P('fs')
All inputs are finite; a program needn't handle non-finite values.
Results may differ from a plain program's by a relative error of at most 0.01.
Values may be sent and summed in bfloat16 or wider, within the bound.
A program may use at most 64 MiB of HBM per device.

v0:
```python
import jax
import jax.numpy as jnp
from jax import lax
from jax.sharding import PartitionSpec as P

EPS = 1e-06


def norm_rows(values, gain):
    scale = lax.rsqrt(jnp.mean(values * values, axis=-1, keepdims=True) + EPS)
    return values * scale * gain


def make_folder(normed, pieces):
    return (
        jnp.dot(normed, pieces[0], preferred_element_type=jnp.float32),
        jnp.dot(normed, pieces[1], preferred_element_type=jnp.float32),
    )


def shards(
    tokens,
    merged,
    gain_first,
    gate_first,
    up_first,
    down_first,
    gain_second,
    gate_second,
    up_second,
    down_second,
):
    normed_first = norm_rows(tokens.astype(jnp.float32), gain_first).astype(jnp.bfloat16)
    gate, up = make_folder(
        normed_first,
        (
            lax.all_gather(gate_first, "fs", axis=0, tiled=True),
            lax.all_gather(up_first, "fs", axis=0, tiled=True),
        ),
    )
    hidden = (jax.nn.silu(gate) * up).astype(jnp.bfloat16)
    down_whole = lax.all_gather(down_first, "fs", axis=1, tiled=True)
    partial_value = jnp.dot(hidden, down_whole, preferred_element_type=jnp.float32)
    first_sum = lax.psum(partial_value.astype(jnp.bfloat16), "tp").astype(jnp.float32)
    middle = tokens.astype(jnp.float32) + merged.astype(jnp.float32) + 0.5 * first_sum
    normed_second = norm_rows(middle, gain_second).astype(jnp.bfloat16)
    gate_two, up_two = make_folder(
        normed_second,
        (
            lax.all_gather(gate_second, "fs", axis=0, tiled=True),
            lax.all_gather(up_second, "fs", axis=0, tiled=True),
        ),
    )
    hidden_two = (jax.nn.silu(gate_two) * up_two).astype(jnp.bfloat16)
    down_two = lax.all_gather(down_second, "fs", axis=1, tiled=True)
    partial_two = jnp.dot(hidden_two, down_two, preferred_element_type=jnp.float32)
    second_sum = lax.psum(partial_two.astype(jnp.bfloat16), "tp").astype(jnp.float32)
    return (middle + 0.5 * second_sum).astype(jnp.bfloat16)


def solution(mesh):
    return jax.shard_map(
        shards,
        mesh=mesh,
        in_specs=(
            P("fs", None),
            P("fs", None),
            P(),
            P("fs", "tp"),
            P("fs", "tp"),
            P("tp", "fs"),
            P(),
            P("fs", "tp"),
            P("fs", "tp"),
            P("tp", "fs"),
        ),
        out_specs=P("fs", None),
        check_vma=False,
    )
```

profile of v0, /device:TPU:0, one launch (start us, length us, event | category | flops | bytes accessed | tf_op | source)
XLA Modules:
  0.0 665.2 jit_solution(4083028435205835512)
XLA Ops:
  6.5 0.7 all-gather.7.cloned.1.call-update
  7.3 0.7 all-gather.11.cloned.1.call-update
  8.1 0.7 all-gather.9.cloned.1.call-update
  8.8 1.8 fusion.1
  10.6 90.9 %all-gather.7.cloned.1.call-done = bf16[2048,1408]{1,0:T(8,128)(2,1)} async-done(((bf16[128,1408]{1,0:T(8,128)(2,1)}), bf16[2048,1408]{1,0:T(8,128)(2,1)}) %all-gather.7.cloned.1.call-update) | async-done | bytes 5767184 | tf_op jit(solution)/shard_map/all_gather | solution.py:37
  101.5 7.1 %fusion.8 = f32[384,1408]{1,0:T(8,128)} fusion(bf16[2048,1408]{1,0:T(8,128)(2,1)} %all-gather.7.cloned.1.call-done, bf16[384,2048]{1,0:T(8,128)(2,1)} %param.10, f32[2048]{0:T(1024)} %param.12, f32[384]{0:T(512)S(1)} %add_rsqrt_fusion.1), kind=kOutput, calls=%fused_computation.16 | convolution fusion | flops 2217738240 | bytes 9512448 | tf_op jit(solution)/shard_map/dot_general | solution.py:16
  108.7 102.6 %all-gather.11.cloned.1.call-done = bf16[1408,2048]{1,0:T(8,128)(2,1)} async-done(((bf16[1408,128]{1,0:T(8,128)(2,1)}), bf16[1408,2048]{1,0:T(8,128)(2,1)}) %all-gather.11.cloned.1.call-update) | async-done | bytes 5767184 | tf_op jit(solution)/shard_map/all_gather | solution.py:42
  211.3 89.7 %all-gather.9.cloned.1.call-done = bf16[2048,1408]{1,0:T(8,128)(2,1)} async-done(((bf16[128,1408]{1,0:T(8,128)(2,1)}), bf16[2048,1408]{1,0:T(8,128)(2,1)}) %all-gather.9.cloned.1.call-update) | async-done | bytes 5767184 | tf_op jit(solution)/shard_map/all_gather | solution.py:38
  300.9 11.2 %convolution_convert_fusion.1 = bf16[384,2048]{1,0:T(8,128)(2,1)} fusion(bf16[1408,2048]{1,0:T(8,128)(2,1)} %all-gather.11.cloned.1.call-done, bf16[2048,1408]{1,0:T(8,128)(2,1)} %all-gather.9.cloned.1.call-done, f32[384,1408]{1,0:T(8,128)} %fusion.8, bf16[384,2048]{1,0:T(8,128)(2,1)S(1)} %copy-done, f32[2048]{0:T(1024)S(1)} %copy-done.4, ...), kind=kOutput, calls=%fused_computation.15 | convolution fusion | flops 4436361216 | bytes 16852480 | tf_op jit(solution)/shard_map/dot_general | solution.py:43
  312.2 0.0 all-gather.13.cloned.1.call-start
  312.2 0.5 all-gather.13.cloned.1.call-update
  312.8 0.5 all-gather.15.cloned.1.call-update
  313.4 0.7 all-gather.17.cloned.1.call-update
  314.1 0.2 all-reduce.5.cloned.1.call-start
  314.3 17.0 %all-reduce.3.cloned.1.call-done = bf16[384,2048]{1,0:T(8,128)(2,1)} async-done(((bf16[384,2048]{1,0:T(8,128)(2,1)}), bf16[384,2048]{1,0:T(8,128)(2,1)}) %all-reduce.3.cloned.1.call-update) | async-done | bytes 1572880 | tf_op jit(solution)/shard_map/psum | solution.py:44
  331.3 2.4 multiply_reduce_fusion
  333.8 2.2 multiply_convert_fusion
  336.0 87.8 %all-gather.13.cloned.1.call-done = bf16[2048,1408]{1,0:T(8,128)(2,1)} async-done(((bf16[128,1408]{1,0:T(8,128)(2,1)}), bf16[2048,1408]{1,0:T(8,128)(2,1)}) %all-gather.13.cloned.1.call-update) | async-done | bytes 5767184 | tf_op jit(solution)/shard_map/all_gather | solution.py:50
  423.8 7.1 %fusion.12 = f32[384,1408]{1,0:T(8,128)} fusion(bf16[384,2048]{1,0:T(8,128)(2,1)} %multiply_convert_fusion, bf16[2048,1408]{1,0:T(8,128)(2,1)} %all-gather.13.cloned.1.call-done), kind=kOutput, calls=%fused_computation.21 | convolution fusion | flops 2214592512 | bytes 9502720 | tf_op jit(solution)/shard_map/dot_general | solution.py:16
  430.9 82.9 %all-gather.15.cloned.1.call-done = bf16[2048,1408]{1,0:T(8,128)(2,1)} async-done(((bf16[128,1408]{1,0:T(8,128)(2,1)}), bf16[2048,1408]{1,0:T(8,128)(2,1)}) %all-gather.15.cloned.1.call-update) | async-done | bytes 5767184 | tf_op jit(solution)/shard_map/all_gather | solution.py:51
  513.8 109.7 %all-gather.17.cloned.1.call-done = bf16[1408,2048]{1,0:T(8,128)(2,1)} async-done(((bf16[1408,128]{1,0:T(8,128)(2,1)}), bf16[1408,2048]{1,0:T(8,128)(2,1)}) %all-gather.17.cloned.1.call-update) | async-done | bytes 5767184 | tf_op jit(solution)/shard_map/all_gather | solution.py:55
  623.6 11.7 %convolution_convert_fusion = bf16[384,2048]{1,0:T(8,128)(2,1)} fusion(bf16[1408,2048]{1,0:T(8,128)(2,1)} %all-gather.17.cloned.1.call-done, bf16[384,2048]{1,0:T(8,128)(2,1)} %multiply_convert_fusion, bf16[2048,1408]{1,0:T(8,128)(2,1)} %all-gather.15.cloned.1.call-done, f32[384,1408]{1,0:T(8,128)} %fusion.12), kind=kOutput, calls=%fused_computation.14 | convolution fusion | flops 4433215488 | bytes 16842752 | tf_op jit(solution)/shard_map/dot_general | solution.py:56
  635.3 18.7 %all-reduce.5.cloned.1.call-done = bf16[384,2048]{1,0:T(8,128)(2,1)} async-done(((bf16[384,2048]{1,0:T(8,128)(2,1)}), bf16[384,2048]{1,0:T(8,128)(2,1)}) %all-reduce.5.cloned.1.call-update) | async-done | bytes 1572880 | tf_op jit(solution)/shard_map/psum | solution.py:57
  654.0 4.3 add_convert_fusion
  (20 shorter events, 0.3 us)
Async XLA Ops:
  6.5 95.0 %all-gather.7.cloned.1.call-start = ((), (), s32[]{:S(2)}) async-start(), calls=%async_computation | async-start | bytes 6127616 | tf_op jit(solution)/shard_map/all_gather | solution.py:37
  7.3 204.0 %all-gather.11.cloned.1.call-start = ((), (), s32[]{:S(2)}) async-start(), calls=%async_computation.2 | async-start | bytes 6127616 | tf_op jit(solution)/shard_map/all_gather | solution.py:42
  8.0 292.9 %all-gather.9.cloned.1.call-start = ((), (), s32[]{:S(2)}) async-start(), calls=%async_computation.1 | async-start | bytes 6127616 | tf_op jit(solution)/shard_map/all_gather | solution.py:38
  8.7 322.6 %all-reduce.3.cloned.1.call-start = ((), (), s32[]{:S(2)}) async-start(), calls=%async_computation.3 | async-start | bytes 3145728 | tf_op jit(solution)/shard_map/psum | solution.py:44
  10.6 290.3 %copy-start = (bf16[384,2048]{1,0:T(8,128)(2,1)S(1)}, bf16[384,2048]{1,0:T(8,128)(2,1)}, u32[]{:S(2)}) copy-start(bf16[384,2048]{1,0:T(8,128)(2,1)} %param.10) | copy-start | bytes 4718596
  10.6 290.3 %copy-start.4 = (f32[2048]{0:T(1024)S(1)}, f32[2048]{0:T(1024)}, u32[]{:S(2)}) copy-start(f32[2048]{0:T(1024)} %param.12) | copy-start | bytes 24580
  312.1 19.2 %copy-start.1 = (bf16[384,2048]{1,0:T(8,128)(2,1)S(1)}, bf16[384,2048]{1,0:T(8,128)(2,1)}, u32[]{:S(2)}) copy-start(bf16[384,2048]{1,0:T(8,128)(2,1)} %param.11) | copy-start | bytes 4718596
  312.2 21.6 %copy-start.3 = (f32[2048]{0:T(1024)S(1)}, f32[2048]{0:T(1024)}, u32[]{:S(2)}) copy-start(f32[2048]{0:T(1024)} %param.16) | copy-start | bytes 24580
  312.2 111.7 %all-gather.13.cloned.1.call-start = ((), (), s32[]{:S(2)}) async-start(), calls=%async_computation.4 | async-start | bytes 6127616 | tf_op jit(solution)/shard_map/all_gather | solution.py:50
  312.8 201.1 %all-gather.15.cloned.1.call-start = ((), (), s32[]{:S(2)}) async-start(), calls=%async_computation.5 | async-start | bytes 6127616 | tf_op jit(solution)/shard_map/all_gather | solution.py:51
  313.3 310.2 %all-gather.17.cloned.1.call-start = ((), (), s32[]{:S(2)}) async-start(), calls=%async_computation.6 | async-start | bytes 6127616 | tf_op jit(solution)/shard_map/all_gather | solution.py:55
  314.1 340.0 %all-reduce.5.cloned.1.call-start = ((), (), s32[]{:S(2)}) async-start(), calls=%async_computation.7 | async-start | bytes 3145728 | tf_op jit(solution)/shard_map/psum | solution.py:57
  331.3 2.4 copy-start.2
Sparse Core Ops, SparseCore 0:
  10.0 91.4 all-gather.6
  104.2 106.9 all-gather.10
  213.9 86.9 all-gather.8
  312.3 19.0 all-reduce.2
  333.9 89.9 all-gather.12
  426.4 87.4 all-gather.14
  516.5 106.9 all-gather.16
  635.4 18.5 all-reduce.4
where the time goes:
time: 665 us
  waiting for transfers between devices  603 us (91%)
  matrix products  37.1 us (6%)
  between operations  13.5 us (2%)
  other arithmetic  10.8 us (2%)
    all_gather x1, waiting for transfers between devices, shards(): down_two = lax.all_gather(down_second, 'fs', axis=1, tiled=True)  110 us
    all_gather x1, waiting for transfers between devices, shards(): down_whole = lax.all_gather(down_first, 'fs', axis=1, tiled=True)  103 us
    all_gather x1, waiting for transfers between devices, shards(): lax.all_gather(gate_first, 'fs', axis=0, tiled=True)  90.9 us
    all_gather x1, waiting for transfers between devices, shards(): lax.all_gather(up_first, 'fs', axis=0, tiled=True)  89.7 us
    all_gather x1, waiting for transfers between devices, shards(): lax.all_gather(gate_second, 'fs', axis=0, tiled=True)  87.8 us
    all_gather x1, waiting for transfers between devices, shards(): lax.all_gather(up_second, 'fs', axis=0, tiled=True)  82.9 us
    psum x1, waiting for transfers between devices, shards(): lax.psum(partial_two.astype(jnp.bfloat16), 'tp').astype(jnp.float32)  18.7 us
    psum x1, waiting for transfers between devices, shards(): lax.psum(partial_value.astype(jnp.bfloat16), 'tp').astype(jnp.float32)  17 us
  transfers between devices with their start and end apart: 8, of which 8 were waited for; matrix products, arithmetic and copies ran while one was open for 3% of the time, Pallas kernels for 0%

commit v1 on v0

--- a/solution.py
+++ b/solution.py
@@ -39,7 +39,12 @@
         ),
     )
     hidden = (jax.nn.silu(gate) * up).astype(jnp.bfloat16)
-    down_whole = lax.all_gather(down_first, "fs", axis=1, tiled=True)
+    ring = [down_first]
+    for hop in range(15):
+        ring.append(lax.ppermute(ring[-1], "fs", [(dev, (dev + 1) % 16) for dev in range(16)]))
+    down_whole = jnp.roll(
+        jnp.concatenate(ring[::-1], axis=1), (lax.axis_index("fs") + 1) * ring[0].shape[1], axis=1
+    )
     partial_value = jnp.dot(hidden, down_whole, preferred_element_type=jnp.float32)
     first_sum = lax.psum(partial_value.astype(jnp.bfloat16), "tp").astype(jnp.float32)
     middle = tokens.astype(jnp.float32) + merged.astype(jnp.float32) + 0.5 * first_sum

time: 665 us -> 682 us (1.026)
  local copies, waits for them, and re-layouts: 0.02 us -> 36.4 us
  waiting for transfers between devices: 603 us -> 581 us
    ppermute x0 -> x15, waiting for transfers between devices: none -> 257 us  [shards(): lax.ppermute(ring[-1], 'fs', [(dev, (dev + 1) % 16) for dev in range(16)])]
    all_gather x1 -> x0, waiting for transfers between devices: 103 us -> none  [shards(): down_whole = lax.all_gather(down_first, 'fs', axis=1, tiled=True)]
    all_gather x1, waiting for transfers between devices: 90.9 us -> 0.01 us  [shards(): lax.all_gather(gate_first, 'fs', axis=0, tiled=True)]
    all_gather x1, waiting for transfers between devices: 89.7 us -> 0.01 us  [shards(): lax.all_gather(up_first, 'fs', axis=0, tiled=True)]
    unnamed x10 -> x69, local copies, waits for them, and re-layouts: 0.02 us -> 35.6 us
  transfers between devices with their start and end apart: 8 -> 22, of which waited for: 8 -> 20; matrix products, arithmetic and copies ran while one was open for 3% -> 8% of each run, Pallas kernels for 0% -> 0%
where the time goes in v1:
time: 682 us
  waiting for transfers between devices  581 us (85%)
  matrix products  36.8 us (5%)
  local copies, waits for them, and re-layouts  36.4 us (5%)
  between operations  13.6 us (2%)
  other arithmetic  10.8 us (2%)
    ppermute x15, waiting for transfers between devices, shards(): lax.ppermute(ring[-1], 'fs', [(dev, (dev + 1) % 16) for dev in range(16)])  257 us
    all_gather x1, waiting for transfers between devices, shards(): down_two = lax.all_gather(down_second, 'fs', axis=1, tiled=True)  110 us
    all_gather x1, waiting for transfers between devices, shards(): lax.all_gather(gate_second, 'fs', axis=0, tiled=True)  87.8 us
    all_gather x1, waiting for transfers between devices, shards(): lax.all_gather(up_second, 'fs', axis=0, tiled=True)  82.9 us
    unnamed x69, local copies, waits for them, and re-layouts  35.6 us
    psum x1, waiting for transfers between devices, shards(): lax.psum(partial_value.astype(jnp.bfloat16), 'tp').astype(jnp.float32)  21.9 us
    psum x1, waiting for transfers between devices, shards(): lax.psum(partial_two.astype(jnp.bfloat16), 'tp').astype(jnp.float32)  18.7 us
    dot_general x2, matrix products, make_folder(): jnp.dot(normed, pieces[0], preferred_element_type=jnp.float32)  13.8 us
  transfers between devices with their start and end apart: 22, of which 20 were waited for; matrix products, arithmetic and copies ran while one was open for 8% of the time, Pallas kernels for 0%

profile of v1, /device:TPU:0, one launch (start us, length us, event | category | flops | bytes accessed | tf_op | source)
XLA Modules:
  0.0 681.6 jit_solution(11050914757159950417)
XLA Ops:
  10.3 12.6 %collective-permute-done = bf16[1408,128]{1,0:T(8,128)(2,1)S(1)} collective-permute-done((bf16[1408,128]{1,0:T(8,128)(2,1)}, bf16[1408,128]{1,0:T(8,128)(2,1)S(1)}, u32[]{:S(2)}, u32[]{:S(2)}) %collective-permute-start) | collective-permute-done | bytes 360480 | tf_op jit(solution)/shard_map/ppermute | solution.py:44
  22.9 20.4 %collective-permute-done.1 = bf16[1408,128]{1,0:T(8,128)(2,1)S(1)} collective-permute-done((bf16[1408,128]{1,0:T(8,128)(2,1)S(1)}, bf16[1408,128]{1,0:T(8,128)(2,1)S(1)}, u32[]{:S(2)}, u32[]{:S(2)}) %collective-permute-start.1) | collective-permute-done | bytes 360480 | tf_op jit(solution)/shard_map/ppermute | solution.py:44
  43.4 21.1 %collective-permute-done.2 = bf16[1408,128]{1,0:T(8,128)(2,1)S(1)} collective-permute-done((bf16[1408,128]{1,0:T(8,128)(2,1)S(1)}, bf16[1408,128]{1,0:T(8,128)(2,1)S(1)}, u32[]{:S(2)}, u32[]{:S(2)}) %collective-permute-start.2) | collective-permute-done | bytes 360480 | tf_op jit(solution)/shard_map/ppermute | solution.py:44
  64.5 15.5 %collective-permute-done.3 = bf16[1408,128]{1,0:T(8,128)(2,1)S(1)} collective-permute-done((bf16[1408,128]{1,0:T(8,128)(2,1)S(1)}, bf16[1408,128]{1,0:T(8,128)(2,1)S(1)}, u32[]{:S(2)}, u32[]{:S(2)}) %collective-permute-start.3) | collective-permute-done | bytes 360480 | tf_op jit(solution)/shard_map/ppermute | solution.py:44
  80.0 21.7 %collective-permute-done.4 = bf16[1408,128]{1,0:T(8,128)(2,1)S(1)} collective-permute-done((bf16[1408,128]{1,0:T(8,128)(2,1)S(1)}, bf16[1408,128]{1,0:T(8,128)(2,1)S(1)}, u32[]{:S(2)}, u32[]{:S(2)}) %collective-permute-start.4) | collective-permute-done | bytes 360480 | tf_op jit(solution)/shard_map/ppermute | solution.py:44
  101.7 21.5 %collective-permute-done.5 = bf16[1408,128]{1,0:T(8,128)(2,1)S(1)} collective-permute-done((bf16[1408,128]{1,0:T(8,128)(2,1)S(1)}, bf16[1408,128]{1,0:T(8,128)(2,1)S(1)}, u32[]{:S(2)}, u32[]{:S(2)}) %collective-permute-start.5) | collective-permute-done | bytes 360480 | tf_op jit(solution)/shard_map/ppermute | solution.py:44
  123.2 15.4 %collective-permute-done.6 = bf16[1408,128]{1,0:T(8,128)(2,1)S(1)} collective-permute-done((bf16[1408,128]{1,0:T(8,128)(2,1)S(1)}, bf16[1408,128]{1,0:T(8,128)(2,1)S(1)}, u32[]{:S(2)}, u32[]{:S(2)}) %collective-permute-start.6) | collective-permute-done | bytes 360480 | tf_op jit(solution)/shard_map/ppermute | solution.py:44
  138.7 12.7 %collective-permute-done.7 = bf16[1408,128]{1,0:T(8,128)(2,1)S(1)} collective-permute-done((bf16[1408,128]{1,0:T(8,128)(2,1)S(1)}, bf16[1408,128]{1,0:T(8,128)(2,1)S(1)}, u32[]{:S(2)}, u32[]{:S(2)}) %collective-permute-start.7) | collective-permute-done | bytes 360480 | tf_op jit(solution)/shard_map/ppermute | solution.py:44
  151.4 11.8 %collective-permute-done.8 = bf16[1408,128]{1,0:T(8,128)(2,1)S(1)} collective-permute-done((bf16[1408,128]{1,0:T(8,128)(2,1)S(1)}, bf16[1408,128]{1,0:T(8,128)(2,1)S(1)}, u32[]{:S(2)}, u32[]{:S(2)}) %collective-permute-start.8) | collective-permute-done | bytes 360480 | tf_op jit(solution)/shard_map/ppermute | solution.py:44
  163.2 18.7 %collective-permute-done.9 = bf16[1408,128]{1,0:T(8,128)(2,1)S(1)} collective-permute-done((bf16[1408,128]{1,0:T(8,128)(2,1)S(1)}, bf16[1408,128]{1,0:T(8,128)(2,1)S(1)}, u32[]{:S(2)}, u32[]{:S(2)}) %collective-permute-start.9) | collective-permute-done | bytes 360480 | tf_op jit(solution)/shard_map/ppermute | solution.py:44
  182.7 21.1 %collective-permute-done.10 = bf16[1408,128]{1,0:T(8,128)(2,1)S(1)} collective-permute-done((bf16[1408,128]{1,0:T(8,128)(2,1)S(1)}, bf16[1408,128]{1,0:T(8,128)(2,1)S(1)}, u32[]{:S(2)}, u32[]{:S(2)}) %collective-permute-start.10) | collective-permute-done | bytes 360480 | tf_op jit(solution)/shard_map/ppermute | solution.py:44
  204.5 14.5 %collective-permute-done.11 = bf16[1408,128]{1,0:T(8,128)(2,1)S(1)} collective-permute-done((bf16[1408,128]{1,0:T(8,128)(2,1)S(1)}, bf16[1408,128]{1,0:T(8,128)(2,1)S(1)}, u32[]{:S(2)}, u32[]{:S(2)}) %collective-permute-start.11) | collective-permute-done | bytes 360480 | tf_op jit(solution)/shard_map/ppermute | solution.py:44
  219.8 22.8 %collective-permute-done.12 = bf16[1408,128]{1,0:T(8,128)(2,1)} collective-permute-done((bf16[1408,128]{1,0:T(8,128)(2,1)S(1)}, bf16[1408,128]{1,0:T(8,128)(2,1)}, u32[]{:S(2)}, u32[]{:S(2)}) %collective-permute-start.12) | collective-permute-done | bytes 360480 | tf_op jit(solution)/shard_map/ppermute | solution.py:44
  242.6 16.8 %collective-permute-done.13 = bf16[1408,128]{1,0:T(8,128)(2,1)} collective-permute-done((bf16[1408,128]{1,0:T(8,128)(2,1)}, bf16[1408,128]{1,0:T(8,128)(2,1)}, u32[]{:S(2)}, u32[]{:S(2)}) %collective-permute-start.13) | collective-permute-done | bytes 360480 | tf_op jit(solution)/shard_map/ppermute | solution.py:44
  261.2 10.7 %collective-permute-done.14 = bf16[1408,128]{1,0:T(8,128)(2,1)S(1)} collective-permute-done((bf16[1408,128]{1,0:T(8,128)(2,1)}, bf16[1408,128]{1,0:T(8,128)(2,1)S(1)}, u32[]{:S(2)}, u32[]{:S(2)}) %collective-permute-start.14) | collective-permute-done | bytes 360480 | tf_op jit(solution)/shard_map/ppermute | solution.py:44
  306.0 6.7 fusion.13
  312.7 11.3 %fusion.8 = bf16[384,2048]{1,0:T(8,128)(2,1)} fusion(bf16[1408,4096]{1,0:T(8,128)(2,1)} %constant_dynamic-update-slice_fusion, s32[]{:T(128)S(6)} %select_n.14, bf16[2048,1408]{1,0:T(8,128)(2,1)} %all-gather.8.cloned.1.call-done, f32[384,1408]{1,0:T(8,128)} %fusion.13, bf16[384,2048]{1,0:T(8,128)(2,1)S(1)} %copy-done, f32[2048]{0:T(1024)S(1)} %copy-done.18, ...), kind=kOutput, calls=%fused_computation.16 | convolution fusion | flops 4436361216 | bytes 16852484 | tf_op jit(solution)/shard_map/dot_general | solution.py:48
  326.0 21.9 %all-reduce.3.cloned.1.call-done = bf16[384,2048]{1,0:T(8,128)(2,1)} async-done(((bf16[384,2048]{1,0:T(8,128)(2,1)}), bf16[384,2048]{1,0:T(8,128)(2,1)}) %all-reduce.3.cloned.1.call-update) | async-done | bytes 1572880 | tf_op jit(solution)/shard_map/psum | solution.py:49
  352.6 87.8 %all-gather.10.cloned.1.call-done = bf16[2048,1408]{1,0:T(8,128)(2,1)} async-done(((bf16[128,1408]{1,0:T(8,128)(2,1)}), bf16[2048,1408]{1,0:T(8,128)(2,1)}) %all-gather.10.cloned.1.call-update) | async-done | bytes 5767184 | tf_op jit(solution)/shard_map/all_gather | solution.py:55
  440.5 7.1 %fusion.18 = f32[384,1408]{1,0:T(8,128)} fusion(bf16[384,2048]{1,0:T(8,128)(2,1)} %multiply_convert_fusion, bf16[2048,1408]{1,0:T(8,128)(2,1)} %all-gather.10.cloned.1.call-done), kind=kOutput, calls=%fused_computation.56 | convolution fusion | flops 2214592512 | bytes 9502720 | tf_op jit(solution)/shard_map/dot_general | solution.py:16
  447.5 82.9 %all-gather.12.cloned.1.call-done = bf16[2048,1408]{1,0:T(8,128)(2,1)} async-done(((bf16[128,1408]{1,0:T(8,128)(2,1)}), bf16[2048,1408]{1,0:T(8,128)(2,1)}) %all-gather.12.cloned.1.call-update) | async-done | bytes 5767184 | tf_op jit(solution)/shard_map/all_gather | solution.py:56
  530.5 109.6 %all-gather.14.cloned.1.call-done = bf16[1408,2048]{1,0:T(8,128)(2,1)} async-done(((bf16[1408,128]{1,0:T(8,128)(2,1)}), bf16[1408,2048]{1,0:T(8,128)(2,1)}) %all-gather.14.cloned.1.call-update) | async-done | bytes 5767184 | tf_op jit(solution)/shard_map/all_gather | solution.py:60
  640.0 11.7 %convolution_convert_fusion = bf16[384,2048]{1,0:T(8,128)(2,1)} fusion(bf16[1408,2048]{1,0:T(8,128)(2,1)} %all-gather.14.cloned.1.call-done, bf16[384,2048]{1,0:T(8,128)(2,1)} %multiply_convert_fusion, bf16[2048,1408]{1,0:T(8,128)(2,1)} %all-gather.12.cloned.1.call-done, f32[384,1408]{1,0:T(8,128)} %fusion.18), kind=kOutput, calls=%fused_computation.17 | convolution fusion | flops 4433215488 | bytes 16842752 | tf_op jit(solution)/shard_map/dot_general | solution.py:61
  651.8 18.7 %all-reduce.5.cloned.1.call-done = bf16[384,2048]{1,0:T(8,128)(2,1)} async-done(((bf16[384,2048]{1,0:T(8,128)(2,1)}), bf16[384,2048]{1,0:T(8,128)(2,1)}) %all-reduce.5.cloned.1.call-update) | async-done | bytes 1572880 | tf_op jit(solution)/shard_map/psum | solution.py:62
  (107 shorter events, 52.9 us)
Async XLA Ops:
  6.5 299.5 %all-gather.6.cloned.1.call-start = ((), (), s32[]{:S(2)}) async-start(), calls=%async_computation | async-start | bytes 6127616 | tf_op jit(solution)/shard_map/all_gather | solution.py:37
  7.3 305.5 %all-gather.8.cloned.1.call-start = ((), (), s32[]{:S(2)}) async-start(), calls=%async_computation.1 | async-start | bytes 6127616 | tf_op jit(solution)/shard_map/all_gather | solution.py:38
  7.3 15.6 %collective-permute-start = (bf16[1408,128]{1,0:T(8,128)(2,1)}, bf16[1408,128]{1,0:T(8,128)(2,1)S(1)}, u32[]{:S(2)}, u32[]{:S(2)}) collective-permute-start(bf16[1408,128]{1,0:T(8,128)(2,1)} %param.15), channel_id=1, source_target_pairs={{0,2},{2,4},{4,6},{6,8},{8,10},{10,12},{12,14},{14,16},{16,18},{18... | collective-permute-start | bytes 1081352 | tf_op jit(solution)/shard_map/ppermute | solution.py:44
  22.9 20.4 %collective-permute-start.1 = (bf16[1408,128]{1,0:T(8,128)(2,1)S(1)}, bf16[1408,128]{1,0:T(8,128)(2,1)S(1)}, u32[]{:S(2)}, u32[]{:S(2)}) collective-permute-start(bf16[1408,128]{1,0:T(8,128)(2,1)S(1)} %collective-permute-done), channel_id=1, source_target_pairs={{0,2},{2,4},{4,6},{6,8},{8,10},{10,12},{12,14},{14,16},{16,18},{18... | collective-permute-start | bytes 1081352 | tf_op jit(solution)/shard_map/ppermute | solution.py:44
  43.4 21.1 %collective-permute-start.2 = (bf16[1408,128]{1,0:T(8,128)(2,1)S(1)}, bf16[1408,128]{1,0:T(8,128)(2,1)S(1)}, u32[]{:S(2)}, u32[]{:S(2)}) collective-permute-start(bf16[1408,128]{1,0:T(8,128)(2,1)S(1)} %collective-permute-done.1), channel_id=1, source_target_pairs={{0,2},{2,4},{4,6},{6,8},{8,10},{10,12},{12,14},{14,16},{16,18},{18... | collective-permute-start | bytes 1081352 | tf_op jit(solution)/shard_map/ppermute | solution.py:44
  64.4 15.5 %collective-permute-start.3 = (bf16[1408,128]{1,0:T(8,128)(2,1)S(1)}, bf16[1408,128]{1,0:T(8,128)(2,1)S(1)}, u32[]{:S(2)}, u32[]{:S(2)}) collective-permute-start(bf16[1408,128]{1,0:T(8,128)(2,1)S(1)} %collective-permute-done.2), channel_id=1, source_target_pairs={{0,2},{2,4},{4,6},{6,8},{8,10},{10,12},{12,14},{14,16},{16,18},{18... | collective-permute-start | bytes 1081352 | tf_op jit(solution)/shard_map/ppermute | solution.py:44
  80.0 21.7 %collective-permute-start.4 = (bf16[1408,128]{1,0:T(8,128)(2,1)S(1)}, bf16[1408,128]{1,0:T(8,128)(2,1)S(1)}, u32[]{:S(2)}, u32[]{:S(2)}) collective-permute-start(bf16[1408,128]{1,0:T(8,128)(2,1)S(1)} %collective-permute-done.3), channel_id=1, source_target_pairs={{0,2},{2,4},{4,6},{6,8},{8,10},{10,12},{12,14},{14,16},{16,18},{18... | collective-permute-start | bytes 1081352 | tf_op jit(solution)/shard_map/ppermute | solution.py:44
  101.7 21.5 %collective-permute-start.5 = (bf16[1408,128]{1,0:T(8,128)(2,1)S(1)}, bf16[1408,128]{1,0:T(8,128)(2,1)S(1)}, u32[]{:S(2)}, u32[]{:S(2)}) collective-permute-start(bf16[1408,128]{1,0:T(8,128)(2,1)S(1)} %collective-permute-done.4), channel_id=1, source_target_pairs={{0,2},{2,4},{4,6},{6,8},{8,10},{10,12},{12,14},{14,16},{16,18},{18... | collective-permute-start | bytes 1081352 | tf_op jit(solution)/shard_map/ppermute | solution.py:44
  123.2 165.2 %copy-start.4 = (bf16[1408,128]{1,0:T(8,128)(2,1)}, bf16[1408,128]{1,0:T(8,128)(2,1)S(1)}, u32[]{:S(2)}) copy-start(bf16[1408,128]{1,0:T(8,128)(2,1)S(1)} %collective-permute-done.5) | copy-start | bytes 1081348
  123.2 15.4 %collective-permute-start.6 = (bf16[1408,128]{1,0:T(8,128)(2,1)S(1)}, bf16[1408,128]{1,0:T(8,128)(2,1)S(1)}, u32[]{:S(2)}, u32[]{:S(2)}) collective-permute-start(bf16[1408,128]{1,0:T(8,128)(2,1)S(1)} %collective-permute-done.5), channel_id=1, source_target_pairs={{0,2},{2,4},{4,6},{6,8},{8,10},{10,12},{12,14},{14,16},{16,18},{18... | collective-permute-start | bytes 1081352 | tf_op jit(solution)/shard_map/ppermute | solution.py:44
  138.7 149.8 %copy-start.6 = (bf16[1408,128]{1,0:T(8,128)(2,1)}, bf16[1408,128]{1,0:T(8,128)(2,1)S(1)}, u32[]{:S(2)}) copy-start(bf16[1408,128]{1,0:T(8,128)(2,1)S(1)} %collective-permute-done.6) | copy-start | bytes 1081348
  138.7 12.7 %collective-permute-start.7 = (bf16[1408,128]{1,0:T(8,128)(2,1)S(1)}, bf16[1408,128]{1,0:T(8,128)(2,1)S(1)}, u32[]{:S(2)}, u32[]{:S(2)}) collective-permute-start(bf16[1408,128]{1,0:T(8,128)(2,1)S(1)} %collective-permute-done.6), channel_id=1, source_target_pairs={{0,2},{2,4},{4,6},{6,8},{8,10},{10,12},{12,14},{14,16},{16,18},{18... | collective-permute-start | bytes 1081352 | tf_op jit(solution)/shard_map/ppermute | solution.py:44
  151.4 11.8 %collective-permute-start.8 = (bf16[1408,128]{1,0:T(8,128)(2,1)S(1)}, bf16[1408,128]{1,0:T(8,128)(2,1)S(1)}, u32[]{:S(2)}, u32[]{:S(2)}) collective-permute-start(bf16[1408,128]{1,0:T(8,128)(2,1)S(1)} %collective-permute-done.7), channel_id=1, source_target_pairs={{0,2},{2,4},{4,6},{6,8},{8,10},{10,12},{12,14},{14,16},{16,18},{18... | collective-permute-start | bytes 1081352 | tf_op jit(solution)/shard_map/ppermute | solution.py:44
  151.4 196.6 %all-reduce.3.cloned.1.call-start = ((), (), s32[]{:S(2)}) async-start(), calls=%async_computation.2 | async-start | bytes 3145728 | tf_op jit(solution)/shard_map/psum | solution.py:49
  163.2 18.7 %collective-permute-start.9 = (bf16[1408,128]{1,0:T(8,128)(2,1)S(1)}, bf16[1408,128]{1,0:T(8,128)(2,1)S(1)}, u32[]{:S(2)}, u32[]{:S(2)}) collective-permute-start(bf16[1408,128]{1,0:T(8,128)(2,1)S(1)} %collective-permute-done.8), channel_id=1, source_target_pairs={{0,2},{2,4},{4,6},{6,8},{8,10},{10,12},{12,14},{14,16},{16,18},{18... | collective-permute-start | bytes 1081352 | tf_op jit(solution)/shard_map/ppermute | solution.py:44
  182.7 21.1 %collective-permute-start.10 = (bf16[1408,128]{1,0:T(8,128)(2,1)S(1)}, bf16[1408,128]{1,0:T(8,128)(2,1)S(1)}, u32[]{:S(2)}, u32[]{:S(2)}) collective-permute-start(bf16[1408,128]{1,0:T(8,128)(2,1)S(1)} %collective-permute-done.9), channel_id=1, source_target_pairs={{0,2},{2,4},{4,6},{6,8},{8,10},{10,12},{12,14},{14,16},{16,18},{18... | collective-permute-start | bytes 1081352 | tf_op jit(solution)/shard_map/ppermute | solution.py:44
  204.5 14.5 %collective-permute-start.11 = (bf16[1408,128]{1,0:T(8,128)(2,1)S(1)}, bf16[1408,128]{1,0:T(8,128)(2,1)S(1)}, u32[]{:S(2)}, u32[]{:S(2)}) collective-permute-start(bf16[1408,128]{1,0:T(8,128)(2,1)S(1)} %collective-permute-done.10), channel_id=1, source_target_pairs={{0,2},{2,4},{4,6},{6,8},{8,10},{10,12},{12,14},{14,16},{16,18},{18... | collective-permute-start | bytes 1081352 | tf_op jit(solution)/shard_map/ppermute | solution.py:44
  219.8 22.8 %collective-permute-start.12 = (bf16[1408,128]{1,0:T(8,128)(2,1)S(1)}, bf16[1408,128]{1,0:T(8,128)(2,1)}, u32[]{:S(2)}, u32[]{:S(2)}) collective-permute-start(bf16[1408,128]{1,0:T(8,128)(2,1)S(1)} %collective-permute-done.11), channel_id=1, source_target_pairs={{0,2},{2,4},{4,6},{6,8},{8,10},{10,12},{12,14},{14,16},{16,18},{18... | collective-permute-start | bytes 1081352 | tf_op jit(solution)/shard_map/ppermute | solution.py:44
  242.6 16.8 %collective-permute-start.13 = (bf16[1408,128]{1,0:T(8,128)(2,1)}, bf16[1408,128]{1,0:T(8,128)(2,1)}, u32[]{:S(2)}, u32[]{:S(2)}) collective-permute-start(bf16[1408,128]{1,0:T(8,128)(2,1)} %collective-permute-done.12), channel_id=1, source_target_pairs={{0,2},{2,4},{4,6},{6,8},{8,10},{10,12},{12,14},{14,16},{16,18},{18... | collective-permute-start | bytes 1081352 | tf_op jit(solution)/shard_map/ppermute | solution.py:44
  259.4 12.5 %collective-permute-start.14 = (bf16[1408,128]{1,0:T(8,128)(2,1)}, bf16[1408,128]{1,0:T(8,128)(2,1)S(1)}, u32[]{:S(2)}, u32[]{:S(2)}) collective-permute-start(bf16[1408,128]{1,0:T(8,128)(2,1)} %collective-permute-done.13), channel_id=1, source_target_pairs={{0,2},{2,4},{4,6},{6,8},{8,10},{10,12},{12,14},{14,16},{16,18},{18... | collective-permute-start | bytes 1081352 | tf_op jit(solution)/shard_map/ppermute | solution.py:44
  324.1 116.4 %all-gather.10.cloned.1.call-start = ((), (), s32[]{:S(2)}) async-start(), calls=%async_computation.3 | async-start | bytes 6127616 | tf_op jit(solution)/shard_map/all_gather | solution.py:55
  324.6 205.8 %all-gather.12.cloned.1.call-start = ((), (), s32[]{:S(2)}) async-start(), calls=%async_computation.4 | async-start | bytes 6127616 | tf_op jit(solution)/shard_map/all_gather | solution.py:56
  325.2 314.8 %all-gather.14.cloned.1.call-start = ((), (), s32[]{:S(2)}) async-start(), calls=%async_computation.5 | async-start | bytes 6127616 | tf_op jit(solution)/shard_map/all_gather | solution.py:60
  325.8 344.7 %all-reduce.5.cloned.1.call-start = ((), (), s32[]{:S(2)}) async-start(), calls=%async_computation.6 | async-start | bytes 3145728 | tf_op jit(solution)/shard_map/psum | solution.py:62
  (17 other events, 470.8 us)
Sparse Core Ops, SparseCore 0:
  10.0 118.7 all-gather.5
  151.5 108.7 all-gather.7
  324.2 23.7 all-reduce.2
  350.5 89.9 all-gather.9
  443.0 87.4 all-gather.11
  533.0 106.9 all-gather.13
  651.9 18.5 all-reduce.4
